TPU v7x, 32 devices: a whole 2x2x4 slice. The times are simulated.
32 devices in a mesh: kv: 8 (over z, x), tp: 4 (over y, core).
Axes of the slice: x: 2, y: 2, z: 4, core: 2. Of those that a mesh axis runs over, the one named last changes fastest.
Arguments:
- tokens: bfloat16 [18, 4096], P(None, ('kv', 'tp')), may hold values from -12.2 to 12.2
- norm_gains: float32 [6, 4096], replicated, may hold values from 0.1 to 1.9
- first_gate: bfloat16 [4096, 11264], P(None, ('kv', 'tp')), may hold values from -0.09375 to 0.09375
- first_lift: bfloat16 [4096, 11264], P(None, ('kv', 'tp')), may hold values from -0.09375 to 0.09375
- first_down: bfloat16 [11264, 4096], P(('kv', 'tp')), may hold values from -0.109375 to 0.109375
- query_weight: bfloat16 [4096, 4096], P('kv', 'tp'), may hold values from -0.09375 to 0.09375
- key_weight: bfloat16 [4096, 4096], P('kv', 'tp'), may hold values from -0.09375 to 0.09375
- value_weight: bfloat16 [4096, 4096], P('kv', 'tp'), may hold values from -0.09375 to 0.09375
- forget_weight: bfloat16 [4096, 64], P(None, 'tp'), may hold values from -0.25 to 0.25
- output_weight: bfloat16 [4096, 4096], P('tp', 'kv'), may hold values from -0.09375 to 0.09375
- second_gate: bfloat16 [4096, 11264], P(None, ('kv', 'tp')), may hold values from -0.09375 to 0.09375
- second_lift: bfloat16 [4096, 11264], P(None, ('kv', 'tp')), may hold values from -0.09375 to 0.09375
- second_down: bfloat16 [11264, 4096], P(('kv', 'tp')), may hold values from -0.109375 to 0.109375
- cache_keys: bfloat16 [18, 2048, 4096], P(None, 'kv', 'tp'), may hold values from -457 to 457
- cache_values: bfloat16 [18, 2048, 4096], P(None, 'kv', 'tp'), may hold values from -6 to 6
- cache_decay: float32 [18, 64, 2048], P(None, 'tp', 'kv'), may hold values from -2500 to 0, as said below
Outputs:
- layer_out: bfloat16 [18, 4096], P(None, ('kv', 'tp'))
Inputs may be any that keep to these rules, and one draw needn't show every extreme that they name: `cache_decay`: each entry is a sum of log forget gates, each at most zero, of the later cached positions of the same sequence and head, so entries never fall along positions and the last is zero.
All inputs are finite; a program needn't handle non-finite values.
Results may differ from a plain program's by a relative error of at most 0.025.
Values may be sent and summed in bfloat16 or wider, within the bound.
A program may use at most 128 MiB of HBM per device.

v0:
```python
import jax
import jax.numpy as jnp
from jax import lax
from jax.sharding import PartitionSpec as P

HD = 64


epsilon = 1e-06


def root_norm(values, norm_gain):
    return (
        values * lax.rsqrt(jnp.mean(values * values, axis=-1, keepdims=True) + epsilon) * norm_gain
    )


def settle(values):
    return lax.optimization_barrier(values.astype(jnp.bfloat16)).astype(jnp.float32)


def gated_terms(stream, pre_gain, gate_matrix, lift_matrix, down_matrix):
    normed = root_norm(stream, pre_gain).astype(jnp.bfloat16)
    gate_part = jnp.dot(normed, gate_matrix, preferred_element_type=jnp.float32)
    lift_part = jnp.dot(normed, lift_matrix, preferred_element_type=jnp.float32)
    active = (jax.nn.silu(gate_part) * lift_part).astype(jnp.bfloat16)
    return jnp.dot(active, down_matrix, preferred_element_type=jnp.float32)


def branch_total(partial_value):
    summed = lax.psum(partial_value, ("kv", "tp"))
    return summed


def spread_heads(per_head):
    return jnp.repeat(per_head, HD, axis=-1)


def absorb(carried, pieces):
    summit, weight_sum, out_sum = carried
    piece_peak, piece_total, piece_out = pieces
    new_summit = jnp.maximum(summit, jnp.max(piece_peak, axis=0))
    kept_share = jnp.exp(summit - new_summit)
    piece_weight = piece_total * jnp.exp(piece_peak - new_summit[None])
    weight_sum = weight_sum * kept_share + jnp.sum(piece_weight, axis=0)
    out_sum = out_sum * spread_heads(kept_share) + jnp.sum(
        spread_heads(piece_weight) * piece_out, axis=0
    )
    return (new_summit, weight_sum, out_sum)


def body(
    tokens,
    norm_gains,
    first_gate,
    first_lift,
    first_down,
    query_weight,
    key_weight,
    value_weight,
    forget_weight,
    output_weight,
    second_gate,
    second_lift,
    second_down,
    cache_keys,
    cache_values,
    cache_decay,
):
    seq_count = tokens.shape[0]
    own_width = tokens.shape[1]
    own_start = lax.axis_index(("kv", "tp")) * own_width
    stream = lax.all_gather(tokens, ("kv", "tp"), axis=1, tiled=True).astype(jnp.float32)
    first_sum = branch_total(gated_terms(stream, norm_gains[0], first_gate, first_lift, first_down))
    first_branch = settle(first_sum)
    middle = stream + 0.5 * root_norm(first_branch, norm_gains[1])
    normed = root_norm(middle, norm_gains[2]).astype(jnp.bfloat16)
    block_rows = query_weight.shape[0]
    feature_block = lax.dynamic_slice_in_dim(
        normed, lax.axis_index("kv") * block_rows, block_rows, 1
    )
    query_part = jnp.dot(feature_block, query_weight, preferred_element_type=jnp.float32)
    key_part = jnp.dot(feature_block, key_weight, preferred_element_type=jnp.float32)
    value_part = jnp.dot(feature_block, value_weight, preferred_element_type=jnp.float32)
    queries, key_new, value_new = (
        lax.psum(query_part.astype(jnp.bfloat16), "kv").astype(jnp.float32),
        lax.psum(key_part.astype(jnp.bfloat16), "kv").astype(jnp.float32),
        lax.psum(value_part.astype(jnp.bfloat16), "kv").astype(jnp.float32),
    )
    queries = queries.astype(jnp.bfloat16)
    key_new = key_new.astype(jnp.bfloat16)
    value_new = value_new.astype(jnp.bfloat16)
    forget = jax.nn.log_sigmoid(jnp.dot(normed, forget_weight, preferred_element_type=jnp.float32))
    head_count = forget_weight.shape[1]
    position_index = cache_keys.shape[1]
    score_scale = HD ** (-0.5)
    query_heads = queries.reshape(seq_count, head_count, HD)
    key_heads = cache_keys.reshape(seq_count, position_index, head_count, HD)
    value_heads = cache_values.reshape(seq_count, position_index, head_count, HD)
    scores = (
        jnp.einsum("bhd,bphd->bhp", query_heads, key_heads, preferred_element_type=jnp.float32)
        * score_scale
    )
    scores = scores + forget[:, :, None] + cache_decay
    block_peak = jnp.max(scores, axis=2)
    raised = jnp.exp(scores - block_peak[:, :, None])
    block_total = jnp.sum(raised, axis=2)
    weighted = jnp.einsum(
        "bhp,bphd->bhd",
        raised.astype(jnp.bfloat16),
        value_heads,
        preferred_element_type=jnp.float32,
    )
    block_out = settle(weighted / block_total[:, :, None]).reshape(seq_count, head_count * HD)
    own_score = (
        jnp.einsum(
            "bhd,bhd->bh",
            query_heads,
            key_new.reshape(seq_count, head_count, HD),
            preferred_element_type=jnp.float32,
        )
        * score_scale
    )
    own_part = (own_score, jnp.ones_like(own_score), value_new.astype(jnp.float32))
    summit, weight_sum, out_sum = absorb(
        own_part,
        (
            lax.all_gather(block_peak[None].astype(jnp.bfloat16), "kv", axis=0, tiled=True).astype(
                jnp.float32
            ),
            lax.all_gather(block_total[None].astype(jnp.bfloat16), "kv", axis=0, tiled=True).astype(
                jnp.float32
            ),
            lax.all_gather(block_out[None].astype(jnp.bfloat16), "kv", axis=0, tiled=True).astype(
                jnp.float32
            ),
        ),
    )
    attended = (out_sum / spread_heads(weight_sum)).astype(jnp.bfloat16)
    projected = settle(jnp.dot(attended, output_weight, preferred_element_type=jnp.float32))
    mixed_block = lax.psum(projected.astype(jnp.bfloat16), "tp")
    mixed_rows = lax.all_gather(mixed_block, "kv", axis=1, tiled=True).astype(jnp.float32)
    after_mix = middle + root_norm(mixed_rows, norm_gains[3])
    second_sum = branch_total(
        gated_terms(after_mix, norm_gains[4], second_gate, second_lift, second_down)
    )
    own_rows = lax.dynamic_slice_in_dim(after_mix, own_start, own_width, 1)
    second_branch = lax.dynamic_slice_in_dim(
        root_norm(settle(second_sum), norm_gains[5]), own_start, own_width, 1
    )
    return (own_rows + 0.5 * second_branch).astype(jnp.bfloat16)


def solution(mesh):
    return jax.shard_map(
        body,
        mesh=mesh,
        in_specs=(
            P(None, ("kv", "tp")),
            P(),
            P(None, ("kv", "tp")),
            P(None, ("kv", "tp")),
            P(("kv", "tp"), None),
            P("kv", "tp"),
            P("kv", "tp"),
            P("kv", "tp"),
            P(None, "tp"),
            P("tp", "kv"),
            P(None, ("kv", "tp")),
            P(None, ("kv", "tp")),
            P(("kv", "tp"), None),
            P(None, "kv", "tp"),
            P(None, "kv", "tp"),
            P(None, "tp", "kv"),
        ),
        out_specs=P(None, ("kv", "tp")),
        check_vma=False,
    )
```

profile of v0, /device:TPU:0, one launch (start us, length us, event | category | flops | bytes accessed | tf_op | source)
XLA Modules:
  0.0 381.9 jit_solution(331709885351848740)
XLA Ops:
  6.5 44.1 %all_gather.15 = bf16[18,4096]{1,0:T(8,128)(2,1)S(1)} all-gather(bf16[18,128]{1,0:T(8,128)(2,1)} %param.16), channel_id=1, replica_groups=mesh['kv'=8,'tp'=4] {'kv','tp'}, dimensions={1}, use_global_device_ids=true | all-gather | bytes 152064 | tf_op jit(solution)/shard_map/all_gather | solution.py:73
  50.9 2.2 fusion.58
  53.1 3.3 fusion.25
  56.4 3.8 fusion.3
  60.2 41.3 %all-reduce.6 = bf16[18,4096]{1,0:T(8,128)(2,1)S(1)} all-reduce(f32[18,4096]{1,0:T(8,128)S(1)} %fusion.3), channel_id=1, replica_groups=mesh['kv'=8,'tp'=4] {'kv','tp'}, use_global_device_ids=true, to_apply=%region_1.2 | all-reduce | flops 73728 | bytes 442368 | tf_op jit(solution)/shard_map/psum | solution.py:31
  101.7 0.3 multiply_reduce_fusion.3
  102.2 1.5 convolution_convert_fusion.1
  103.7 0.8 reshape.104
  104.5 0.2 convolution_convert_fusion
  104.7 0.8 reshape.105
  105.5 0.9 convolution_convert_fusion.2
  106.6 12.7 %copy.36 = bf16[18,256,1024]{1,2,0:T(8,128)(2,1)} copy(bf16[18,256,1024]{2,1,0:T(8,128)(2,1)} %param.29) | data formatting | bytes 18874368 | tf_op args[13]
  119.4 12.7 %copy.42 = bf16[18,256,1024]{1,2,0:T(8,128)(2,1)} copy(bf16[18,256,1024]{2,1,0:T(8,128)(2,1)} %param.30) | data formatting | bytes 18874368 | tf_op args[14]
  132.0 0.7 dynamic-slice
  132.8 44.2 %all-reduce.5.cloned.1.call-done = (bf16[18,16,64]{2,1,0:T(8,128)(2,1)}, bf16[18,16,64]{2,1,0:T(8,128)(2,1)}, bf16[18,1024]{1,0:T(8,128)(2,1)}) async-done(((bf16[18,16,64]{2,1,0:T(8,128)(2,1)}, bf16[18,16,64]{2,1,0:T(8,128)(2,1)}, bf16[18,1024]{1,0:T(8,128)(2,1)}), (bf16[18,16,64]{2,1,0:T(8,128)(2,1)}, bf16[18,16,64]{2,1,0:T(8,128)(2,1)}, bf16[18,1024]{1,0:T(8,128)(2,1)})) %all-reduce.5.cloned.1.call-update) | async-done | bytes 110608 | tf_op jit(solution)/shard_map/psum | solution.py:86
  177.0 5.2 %fusion.21 = f32[18,16,1,256]{3,2,1,0:T(1,128)S(1)} fusion(bf16[18,256,16,64]{1,3,2,0:T(8,128)(2,1)} %bitcast.42, bf16[18,16,64,1]{2,1,0,3:T(8,128)(2,1)} %bitcast.44), kind=kOutput, calls=%fused_computation.44 | convolution fusion | flops 9437184 | bytes 9768960 | tf_op jit(solution)/shard_map/bhd,bphd->bhp/dot_general | solution.py:101
  182.6 0.9 copy-done.2
  183.5 2.5 fusion.15
  186.2 31.2 %all_gather.18 = bf16[8,18,1024]{2,1,0:T(8,128)(2,1)S(1)} all-gather(bf16[1,18,1024]{2,1,0:T(8,128)(2,1)S(1)} %convert_element_type.136), channel_id=1, replica_groups=mesh['kv'=8,'tp'=4] {'kv'}, dimensions={0}, use_global_device_ids=true | all-gather | bytes 331776 | tf_op jit(solution)/shard_map/all_gather | solution.py:134
  217.5 30.6 %all-gather.3 = bf16[8,18,16]{1,2,0:T(8,128)(2,1)S(1)} all-gather(bf16[1,18,16]{1,2,0:T(8,128)(2,1)S(1)} %copy.40), channel_id=3, replica_groups=mesh['kv'=8,'tp'=4] {'kv'}, dimensions={0}, use_global_device_ids=true | all-gather | bytes 5184 | tf_op jit(solution)/shard_map/all_gather | solution.py:131
  248.2 30.6 %all-gather.2 = bf16[8,18,16]{1,2,0:T(8,128)(2,1)S(1)} all-gather(bf16[1,18,16]{1,2,0:T(8,128)(2,1)S(1)} %copy.38), channel_id=2, replica_groups=mesh['kv'=8,'tp'=4] {'kv'}, dimensions={0}, use_global_device_ids=true | all-gather | bytes 5184 | tf_op jit(solution)/shard_map/all_gather | solution.py:128
  279.2 0.4 broadcast_in_dim.7
  279.6 0.3 reshape.108
  280.5 0.3 multiply_reduce_fusion
  280.9 1.5 convolution_convert_fusion.3
  282.4 10.3 %psum.46 = bf16[18,512]{1,0:T(8,128)(2,1)S(1)} all-reduce(bf16[18,512]{1,0:T(8,128)(2,1)S(1)} %convolution_convert_fusion.3), channel_id=1, replica_groups=mesh['kv'=8,'tp'=4] {'tp'}, use_global_device_ids=true, to_apply=%region_12.13 | all-reduce | flops 9216 | bytes 36864 | tf_op jit(solution)/shard_map/psum | solution.py:141
  292.6 30.8 %all_gather.19 = bf16[18,4096]{1,0:T(8,128)(2,1)S(1)} all-gather(bf16[18,512]{1,0:T(8,128)(2,1)S(1)} %psum.46), channel_id=1, replica_groups=mesh['kv'=8,'tp'=4] {'kv'}, dimensions={1}, use_global_device_ids=true | all-gather | bytes 165888 | tf_op jit(solution)/shard_map/all_gather | solution.py:142
  323.6 0.3 multiply_reduce_fusion.2
  324.0 2.8 fusion.52
  326.8 5.5 %fusion.2 = f32[18,4096]{1,0:T(8,128)} fusion(bf16[352,4096]{1,0:T(8,128)(2,1)} %param.28, bf16[4096,352]{0,1:T(8,128)(2,1)} %param.27, f32[18,352]{1,0:T(8,128)S(1)} %fusion.52, f32[18,4096]{1,0:T(8,128)S(1)} %get-tuple-element.9, f32[4096]{0:T(1024)S(1)} %bitcast.49, f32[18]{0:T(128)S(1)} %add_rsqrt_fusion.1), kind=kOutput, calls=%fused_computation.8 | convolution fusion | flops 104068224 | bytes 6398792 | tf_op jit(solution)/shard_map/dot_general | solution.py:27
  332.2 41.9 %all-reduce.7 = bf16[18,4096]{1,0:T(8,128)(2,1)S(1)} all-reduce(f32[18,4096]{1,0:T(8,128)} %fusion.2), channel_id=1, replica_groups=mesh['kv'=8,'tp'=4] {'kv','tp'}, use_global_device_ids=true, to_apply=%region_15.16 | all-reduce | flops 73728 | bytes 442368 | tf_op jit(solution)/shard_map/psum | solution.py:31
  374.3 0.7 fusion.45
  (58 shorter events, 3.0 us)
Async XLA Ops:
  6.5 49.8 %copy-start = (bf16[352,4096]{1,0:T(8,128)(2,1)S(1)}, bf16[352,4096]{1,0:T(8,128)(2,1)}, u32[]{:S(2)}) copy-start(bf16[352,4096]{1,0:T(8,128)(2,1)} %param.20) | copy-start | bytes 8650756
  6.5 170.4 %all-reduce.5.cloned.1.call-start = ((), (), s32[]{:S(2)}) async-start(), calls=%async_computation | async-start | bytes 393216 | tf_op jit(solution)/shard_map/psum | solution.py:86
  50.8 2.2 copy-start.10
  60.2 44.3 %copy-start.4 = (bf16[512,1024]{1,0:T(8,128)(2,1)S(1)}, bf16[512,1024]{1,0:T(8,128)(2,1)}, u32[]{:S(2)}) copy-start(bf16[512,1024]{1,0:T(8,128)(2,1)} %param.22) | copy-start | bytes 3145732
  60.2 45.3 %copy-start.5 = (bf16[512,1024]{1,0:T(8,128)(2,1)S(1)}, bf16[512,1024]{1,0:T(8,128)(2,1)}, u32[]{:S(2)}) copy-start(bf16[512,1024]{1,0:T(8,128)(2,1)} %param.23) | copy-start | bytes 3145732
  60.2 46.2 %copy-start.7 = (bf16[4096,16]{0,1:T(8,128)(2,1)S(1)}, bf16[4096,16]{0,1:T(8,128)(2,1)}, u32[]{:S(2)}) copy-start(bf16[4096,16]{0,1:T(8,128)(2,1)} %param.24) | copy-start | bytes 393220
  176.9 5.2 %copy-start.6 = (f32[18,16,256]{2,1,0:T(8,128)S(1)}, f32[18,16,256]{2,1,0:T(8,128)}, u32[]{:S(2)}) copy-start(f32[18,16,256]{2,1,0:T(8,128)} %param.31) | copy-start | bytes 884740
  176.9 6.5 %copy-start.2 = (bf16[18,256,1024]{1,2,0:T(8,128)(2,1)S(1)}, bf16[18,256,1024]{1,2,0:T(8,128)(2,1)}, u32[]{:S(2)}) copy-start(bf16[18,256,1024]{1,2,0:T(8,128)(2,1)} %copy.42) | copy-start | bytes 28311556
  183.5 95.4 %copy-start.3 = (bf16[18,16,64]{2,1,0:T(8,128)(2,1)S(1)}, bf16[18,16,64]{2,1,0:T(8,128)(2,1)}, u32[]{:S(2)}) copy-start(bf16[18,16,64]{2,1,0:T(8,128)(2,1)} %get-tuple-element.5) | copy-start | bytes 110596
  183.5 95.4 %copy-start.8 = (bf16[18,16,64]{2,1,0:T(8,128)(2,1)S(1)}, bf16[18,16,64]{2,1,0:T(8,128)(2,1)}, u32[]{:S(2)}) copy-start(bf16[18,16,64]{2,1,0:T(8,128)(2,1)} %get-tuple-element.6) | copy-start | bytes 110596
  217.4 63.4 %copy-start.9 = (bf16[18,1024]{1,0:T(8,128)(2,1)S(1)}, bf16[18,1024]{1,0:T(8,128)(2,1)}, u32[]{:S(2)}) copy-start(bf16[18,1024]{1,0:T(8,128)(2,1)} %get-tuple-element.7) | copy-start | bytes 110596
  324.0 51.1 %copy-start.1 = (bf16[352,4096]{1,0:T(8,128)(2,1)S(1)}, bf16[352,4096]{1,0:T(8,128)(2,1)}, u32[]{:S(2)}) copy-start(bf16[352,4096]{1,0:T(8,128)(2,1)} %param.20) | copy-start | bytes 8650756
Sparse Core Ops, SparseCore 0:
  106.5 70.3 all-reduce.4
where the time goes:
time: 383 us; the launch traced here: 382 us
  blocking collectives  261 us (68%)
  waiting for transfers between devices  44.2 us (12%)
  local copies, waits for them, and re-layouts  32.6 us (9%)
  matrix products  27.4 us (7%)
  between operations  13.6 us (4%)
    psum x2, blocking collectives, branch_total(): summed = lax.psum(partial_value, ('kv', 'tp'))  83.2 us
    psum x1, waiting for transfers between devices, body(): lax.psum(query_part.astype(jnp.bfloat16), 'kv').astype(jnp.float32)  44.2 us
    all_gather x1, blocking collectives, body(): lax.all_gather(tokens, ('kv', 'tp'), axis=1, tiled=True).astype(jnp.float32)  44.1 us
    all_gather x1, blocking collectives, body(): lax.all_gather(block_out[None].astype(jnp.bfloat16), 'kv', axis=0, tiled=...  31.2 us
    all_gather x1, blocking collectives, body(): lax.all_gather(mixed_block, 'kv', axis=1, tiled=True).astype(jnp.float32)  30.8 us
    all_gather x1, blocking collectives, body(): lax.all_gather(block_total[None].astype(jnp.bfloat16), 'kv', axis=0, tile...  30.6 us
    all_gather x1, blocking collectives, body(): lax.all_gather(block_peak[None].astype(jnp.bfloat16), 'kv', axis=0, tiled...  30.6 us
    unnamed x26, local copies, waits for them, and re-layouts  26.4 us
  transfers between devices with their start and end apart: 1, of which 1 were waited for; matrix products, arithmetic and copies ran while one was open for 7% of the time, Pallas kernels for 0%

commit v1 on v0

--- a/solution.py
+++ b/solution.py
@@ -1,6 +1,10 @@
+import functools
+
 import jax
 import jax.numpy as jnp
 from jax import lax
+from jax.experimental import pallas as pl
+from jax.experimental.pallas import tpu as pltpu
 from jax.sharding import PartitionSpec as P
 
 HD = 64
@@ -151,9 +155,289 @@
     return (own_rows + 0.5 * second_branch).astype(jnp.bfloat16)
 
 
+MESH = pl.DeviceIdType.MESH
+F32 = jnp.float32
+BF16 = jnp.bfloat16
+
+
+def wide_dot(a, b):
+    return lax.dot_general(a, b, (((1,), (1,)), ((), ())), preferred_element_type=F32)
+
+
+def fused_kernel(n_kv, n_tp, *refs):
+    n = n_kv * n_tp
+    (tokens, gains, *hbm_refs) = refs[:16]
+    out = refs[16]
+    vmem_refs = refs[17:31]
+    (
+        x2d, stage, nrm, mid, part_sum, q2d, o2d, l2d,
+        xbuf, send_all, recv_all, own_all, bbuf, mbuf, recv_two, tbuf,
+        send_qkv, recv_qkv, own_kv, qbuf, send_part, recv_part,
+        send_lse, recv_lse, abuf, send_tp, recv_tp,
+        load_sem, all_send, all_recv, kv_send, kv_recv, tp_send, tp_recv,
+    ) = refs[31:]
+    (
+        g1, l1, d1, wq, wk, wv, wf, wo, g2, l2, d2, ck, cv, cd
+    ) = vmem_refs
+    rows, c = tokens.shape
+    depth = n * c
+    kv = lax.axis_index("kv")
+    tp = lax.axis_index("tp")
+    me = kv * n_tp + tp
+
+    order = (0, 1, 2, 3, 4, 5, 6, 11, 13, 12, 7, 8, 9, 10)
+    loads = [
+        pltpu.make_async_copy(hbm_refs[i], vmem_refs[i], load_sem.at[i]) for i in range(14)
+    ]
+    for i in order:
+        loads[i].start()
+
+    barrier = pltpu.get_barrier_semaphore()
+
+    @pl.loop(1, n)
+    def _(k):
+        peer = lax.rem(me + k, n)
+        pl.semaphore_signal(
+            barrier, inc=1, device_id=(lax.div(peer, n_tp), lax.rem(peer, n_tp)),
+            device_id_type=MESH,
+        )
+
+    pl.semaphore_wait(barrier, n - 1)
+
+    def group(axis):
+        if axis == "all":
+            return n, me, lambda p: (lax.div(p, n_tp), lax.rem(p, n_tp)), all_send, all_recv
+        if axis == "kv":
+            return n_kv, kv, lambda p: (p, tp), kv_send, kv_recv
+        return n_tp, tp, lambda p: (kv, p), tp_send, tp_recv
+
+    def remote(src, dst, slot, axis, which, peer, index):
+        size, here, place, send_sem, recv_sem = group(axis)
+        return pltpu.make_async_remote_copy(
+            src_ref=src, dst_ref=dst.at[slot],
+            send_sem=send_sem.at[which, peer], recv_sem=recv_sem.at[which, index],
+            device_id=place(peer), device_id_type=MESH,
+        )
+
+    def exchange(axis, pairs):
+        size, here = group(axis)[:2]
+
+        @pl.loop(1, size)
+        def _(k):
+            peer = lax.rem(here + k, size)
+            for src, dst, which, scattered in pairs:
+                remote(
+                    src.at[peer] if scattered else src, dst, here, axis, which, peer, here
+                ).start()
+
+        for src, dst, which, scattered in pairs:
+            dst[here] = src[here] if scattered else src[...]
+
+        @pl.loop(1, size)
+        def _(k):
+            peer = lax.rem(here + k, size)
+            for src, dst, which, scattered in pairs:
+                remote(
+                    src.at[peer] if scattered else src, dst, peer, axis, which, peer, peer
+                ).wait()
+
+    def flatten(buf, target, count):
+        for i in range(count):
+            target[:, i * c : (i + 1) * c] = buf[i].astype(target.dtype)
+
+    def branch(pre_ref, gate, lift, down, first_load):
+        for i in range(3):
+            loads[first_load + i].wait()
+        hidden = gate.shape[0]
+        step = c * max(1, min(4, n))
+
+        def up(k, carry):
+            a, b = carry
+            ds = pl.ds(pl.multiple_of(k * step, c), step)
+            v = pre_ref[:, ds]
+            a = a + wide_dot(v, gate[:, ds])
+            b = b + wide_dot(v, lift[:, ds])
+            return a, b
+
+        zero = jnp.zeros((rows, hidden), F32)
+        a, b = lax.fori_loop(0, depth // step, up, (zero, zero))
+        active = (a / (1.0 + jnp.exp(-a)) * b).astype(BF16)
+        group_size = step // c
+
+        @pl.loop(0, depth // step)
+        def _(k):
+            ds = pl.ds(pl.multiple_of(k * step, c), step)
+            y = jnp.dot(active, down[:, ds], preferred_element_type=F32).astype(BF16)
+            for j in range(group_size):
+                send_all[k * group_size + j] = y[:, j * c : (j + 1) * c]
+
+    def total(buf, count):
+        acc = buf[0].astype(F32)
+        for i in range(1, count):
+            acc = acc + buf[i].astype(F32)
+        return acc
+
+    exchange("all", [(tokens, xbuf, 0, False)])
+    flatten(xbuf, x2d, n)
+    nrm[...] = root_norm(x2d[...], gains[0:1, :]).astype(BF16)
+    branch(nrm, g1, l1, d1, 0)
+    exchange("all", [(send_all, recv_all, 1, True)])
+    own_all[...] = total(recv_all, n).astype(BF16)
+    exchange("all", [(own_all, bbuf, 2, False)])
+    flatten(bbuf, stage, n)
+    middle = x2d[...] + 0.5 * root_norm(stage[...], gains[1:2, :])
+    mid[...] = middle
+    nrm[...] = root_norm(middle, gains[2:3, :]).astype(BF16)
+
+    for i in (3, 4, 5, 6):
+        loads[i].wait()
+    block_rows = wq.shape[0]
+    block = nrm[:, pl.ds(pl.multiple_of(kv * block_rows, c), block_rows)]
+    for i, w in enumerate((wq, wk, wv)):
+        y = jnp.dot(block, w[...], preferred_element_type=F32).astype(BF16)
+        for j in range(n_kv):
+            send_qkv[j, i] = y[:, j * c : (j + 1) * c]
+    forget_t = jax.nn.log_sigmoid(wide_dot(wf[...], nrm[...]))
+    exchange("kv", [(send_qkv, recv_qkv, 0, True)])
+    qkv = total(recv_qkv, n_kv).astype(BF16)
+    own_kv[...] = qkv[0]
+    exchange("kv", [(own_kv, qbuf, 1, False)])
+    flatten(qbuf, q2d, n_kv)
+
+    for i in (11, 12, 13):
+        loads[i].wait()
+    heads = wf.shape[0]
+    width = heads * HD
+    scale = HD ** (-0.5)
+    head_of = lax.broadcasted_iota(jnp.int32, (heads, width), 1) // HD
+    mask = head_of == lax.broadcasted_iota(jnp.int32, (heads, width), 0)
+
+    for b in range(rows):
+        q = jnp.where(mask, q2d[b : b + 1, :], 0.0).astype(BF16)
+        s = wide_dot(q, ck[b]) * scale + forget_t[:, b : b + 1] + cd[b]
+        peak = jnp.max(s, axis=1, keepdims=True)
+        e = jnp.exp(s - peak)
+        sums = jnp.sum(e, axis=1, keepdims=True)
+        o = jnp.dot(e.astype(BF16), cv[b], preferred_element_type=F32) / sums
+        lse = peak + jnp.log(sums)
+        o2d[b : b + 1, :] = jnp.sum(jnp.where(mask, o, 0.0), axis=0, keepdims=True)
+        l2d[b : b + 1, :] = jnp.sum(jnp.where(mask, lse, 0.0), axis=0, keepdims=True)
+
+    for j in range(n_kv):
+        send_part[j] = o2d[:, j * c : (j + 1) * c].astype(BF16)
+        send_lse[j] = l2d[:, j * c : (j + 1) * c]
+    exchange("kv", [(send_part, recv_part, 2, True), (send_lse, recv_lse, 3, True)])
+    qk = qkv[0].astype(F32) * qkv[1].astype(F32)
+    lane_head = lax.broadcasted_iota(jnp.int32, (rows, c), 1) // HD
+    own = jnp.zeros((rows, c), F32)
+    for h in range(c // HD):
+        mine = lane_head == h
+        own = jnp.where(
+            mine, jnp.sum(jnp.where(mine, qk, 0.0), axis=1, keepdims=True) * scale, own
+        )
+    top = own
+    for j in range(n_kv):
+        top = jnp.maximum(top, recv_lse[j])
+    weight = jnp.exp(own - top)
+    value = weight * qkv[2].astype(F32)
+    for j in range(n_kv):
+        w = jnp.exp(recv_lse[j] - top)
+        weight = weight + w
+        value = value + w * recv_part[j].astype(F32)
+    own_kv[...] = (value / weight).astype(BF16)
+    exchange("kv", [(own_kv, abuf, 4, False)])
+    flatten(abuf, q2d, n_kv)
+    loads[7].wait()
+    y = jnp.dot(q2d[...].astype(BF16), wo[...], preferred_element_type=F32).astype(BF16)
+    for j in range(n_tp):
+        send_tp[j] = y[:, j * c : (j + 1) * c]
+    exchange("tp", [(send_tp, recv_tp, 0, True)])
+    own_all[...] = total(recv_tp, n_tp).astype(BF16)
+    exchange("all", [(own_all, mbuf, 3, False)])
+    flatten(mbuf, stage, n)
+    after = mid[...] + root_norm(stage[...], gains[3:4, :])
+    mid[...] = after
+    nrm[...] = root_norm(after, gains[4:5, :]).astype(BF16)
+    branch(nrm, g2, l2, d2, 8)
+    exchange("all", [(send_all, recv_two, 4, True)])
+    last = total(recv_two, n).astype(BF16)
+    own_all[...] = last
+    exchange("all", [(own_all, tbuf, 5, False)])
+    squares = jnp.zeros((rows, c), F32)
+    for i in range(n):
+        v = tbuf[i].astype(F32)
+        squares = squares + v * v
+    inv = lax.rsqrt(jnp.sum(squares, axis=1, keepdims=True) / depth + epsilon)
+    here = pl.ds(pl.multiple_of(me * c, c), c)
+    out[...] = (mid[:, here] + 0.5 * (last.astype(F32) * inv * gains[5:6, here])).astype(BF16)
+
+
+def layer(n_kv, n_tp, *args):
+    tokens = args[0]
+    rows, c = tokens.shape
+    n = n_kv * n_tp
+    if c % 128 or args[5].shape[1] != n_kv * c or args[9].shape[1] != n_tp * c:
+        return body(*args)
+    depth = n * c
+    width = args[8].shape[1] * HD
+    args = [a.T if i in (2, 3, 8, 10, 11) else a for i, a in enumerate(args)]
+    vmem = pltpu.VMEM
+    chunk = (rows, c)
+    dma = pltpu.SemaphoreType.DMA
+    scratch = [vmem(a.shape, a.dtype) for a in args[2:]]
+    scratch += [
+        vmem((rows, depth), F32),
+        vmem((rows, depth), F32),
+        vmem((rows, depth), BF16),
+        vmem((rows, depth), F32),
+        vmem((8, 128), F32),
+        vmem((rows, width), F32),
+        vmem((rows, width), F32),
+        vmem((rows, width), F32),
+        vmem((n, *chunk), BF16),
+        vmem((n, *chunk), BF16),
+        vmem((n, *chunk), BF16),
+        vmem(chunk, BF16),
+        vmem((n, *chunk), BF16),
+        vmem((n, *chunk), BF16),
+        vmem((n, *chunk), BF16),
+        vmem((n, *chunk), BF16),
+        vmem((n_kv, 3, *chunk), BF16),
+        vmem((n_kv, 3, *chunk), BF16),
+        vmem(chunk, BF16),
+        vmem((n_kv, *chunk), BF16),
+        vmem((n_kv, *chunk), BF16),
+        vmem((n_kv, *chunk), BF16),
+        vmem((n_kv, *chunk), F32),
+        vmem((n_kv, *chunk), F32),
+        vmem((n_kv, *chunk), BF16),
+        vmem((n_tp, *chunk), BF16),
+        vmem((n_tp, *chunk), BF16),
+        dma((14,)),
+        dma((6, n)),
+        dma((6, n)),
+        dma((5, n_kv)),
+        dma((5, n_kv)),
+        dma((1, n_tp)),
+        dma((1, n_tp)),
+    ]
+    anywhere = pl.BlockSpec(memory_space=pl.ANY)
+    inside = pl.BlockSpec(memory_space=pltpu.VMEM)
+    return pl.pallas_call(
+        functools.partial(fused_kernel, n_kv, n_tp),
+        out_shape=jax.ShapeDtypeStruct((rows, c), BF16),
+        in_specs=[inside, inside] + [anywhere] * 14,
+        out_specs=inside,
+        scratch_shapes=scratch,
+        compiler_params=pltpu.CompilerParams(
+            collective_id=0, has_side_effects=True, vmem_limit_bytes=66 * 1000 * 1000
+        ),
+    )(*args)
+
+
 def solution(mesh):
     return jax.shard_map(
-        body,
+        functools.partial(layer, mesh.shape["kv"], mesh.shape["tp"]),
         mesh=mesh,
         in_specs=(
             P(None, ("kv", "tp")),

time: 383 us -> 96 us (0.25)
  blocking collectives: 261 us -> 0 us
  Pallas kernels: 0 us -> 93.9 us
  waiting for transfers between devices: 44.2 us -> 0 us
  local copies, waits for them, and re-layouts: 32.6 us -> 1.29 us
  matrix products: 27.4 us -> 0 us
  between operations: 13.6 us -> 0.01 us
    all_gather x5 -> x0, blocking collectives: 167 us -> none  [the longest x1 44.1 us: body(): lax.all_gather(tokens, ('kv', 'tp'), axis=1, tiled=True).astype(jnp.float32)]
    pallas_call x0 -> x1, Pallas kernels: none -> 93.9 us  [layer(): pl.pallas_call(functools.partial(fused_kernel, n_kv, n_tp), out_shape=jax...]
    psum x3 -> x0, blocking collectives: 93.4 us -> none  [the longest x2 83.2 us: branch_total(): summed = lax.psum(partial_value, ('kv', 'tp'))]
    psum x1 -> x0, waiting for transfers between devices: 44.2 us -> none  [body(): lax.psum(query_part.astype(jnp.bfloat16), 'kv').astype(jnp.float32)]
    dot_general x11 -> x0, matrix products: 27.4 us -> none  [the longest x2 9.27 us: gated_terms(): return jnp.dot(active, down_matrix, preferred_element_type=jnp.float32)]
    unnamed x26 -> x1, local copies, waits for them, and re-layouts: 26.4 us -> 1.29 us
  transfers between devices with their start and end apart: 1 -> 0, of which waited for: 1 -> 0; matrix products, arithmetic and copies ran while one was open for 7% -> 0% of each run, Pallas kernels for 0% -> 0%
where the time goes in v1:
time: 96 us; the launch traced here: 95.2 us
  Pallas kernels  93.9 us (98%)
  local copies, waits for them, and re-layouts  1.29 us (1%)
    pallas_call x1, Pallas kernels, layer(): pl.pallas_call(functools.partial(fused_kernel, n_kv, n_tp), out_shape=jax...  93.9 us

profile of v1, /device:TPU:0, one launch (start us, length us, event | category | flops | bytes accessed | tf_op | source)
XLA Modules:
  0.0 95.2 jit_solution(13037057909909178587)
XLA Ops:
  0.0 93.9 %shard_map.154 = bf16[18,128]{1,0:T(8,128)(2,1)} custom-call(bf16[18,128]{1,0:T(8,128)(2,1)} %refs_0_.1, f32[6,4096]{1,0:T(8,128)} %refs_1_.1, bf16[352,4096]{1,0:T(8,128)(2,1)} %bitcast.5, bf16[352,4096]{1,0:T(8,128)(2,1)} %bitcast.6, bf16[352,4096]{1,0:T(8,128)(2,1)} %refs_4_.1, bf16[512,1024]{1,0:T(8,128)(2,1)} %refs_5_.1, bf16[512,1024]{1,0:T(8,128)(2,1)} %refs_6_.1, ...), custom_call_target="tpu_custom_call" | custom-call | tf_op jit(solution)/shard_map/pallas_call | solution.py:426
  93.9 1.3 %copy.18 = bf16[18,128]{1,0:T(8,128)(2,1)} copy(bf16[18,128]{1,0:T(8,128)(2,1)} %shard_map.154) | data formatting | bytes 9216

commit v2 on v1

--- a/solution.py
+++ b/solution.py
@@ -170,7 +170,7 @@
     out = refs[16]
     vmem_refs = refs[17:31]
     (
-        x2d, stage, nrm, mid, part_sum, q2d, o2d, l2d,
+        x2d, stage, nrm, mid, stat, q2d, o2d, l2d,
         xbuf, send_all, recv_all, own_all, bbuf, mbuf, recv_two, tbuf,
         send_qkv, recv_qkv, own_kv, qbuf, send_part, recv_part,
         send_lse, recv_lse, abuf, send_tp, recv_tp,
@@ -249,7 +249,7 @@
         for i in range(3):
             loads[first_load + i].wait()
         hidden = gate.shape[0]
-        step = c * max(1, min(4, n))
+        step = c * max(1, min(16, n))
 
         def up(k, carry):
             a, b = carry
@@ -312,16 +312,26 @@
     head_of = lax.broadcasted_iota(jnp.int32, (heads, width), 1) // HD
     mask = head_of == lax.broadcasted_iota(jnp.int32, (heads, width), 0)
 
-    for b in range(rows):
-        q = jnp.where(mask, q2d[b : b + 1, :], 0.0).astype(BF16)
-        s = wide_dot(q, ck[b]) * scale + forget_t[:, b : b + 1] + cd[b]
+    lane = lax.broadcasted_iota(jnp.int32, (heads, rows), 1)
+    pace = 3 if rows % 3 == 0 else 1
+
+    def sequence(b):
+        q = jnp.where(mask, q2d[pl.ds(b, 1), :], 0.0).astype(BF16)
+        s = wide_dot(q, ck[b]) * scale + jnp.sum(
+            jnp.where(lane == b, forget_t, 0.0), axis=1, keepdims=True
+        ) + cd[b]
         peak = jnp.max(s, axis=1, keepdims=True)
         e = jnp.exp(s - peak)
         sums = jnp.sum(e, axis=1, keepdims=True)
         o = jnp.dot(e.astype(BF16), cv[b], preferred_element_type=F32) / sums
         lse = peak + jnp.log(sums)
-        o2d[b : b + 1, :] = jnp.sum(jnp.where(mask, o, 0.0), axis=0, keepdims=True)
-        l2d[b : b + 1, :] = jnp.sum(jnp.where(mask, lse, 0.0), axis=0, keepdims=True)
+        o2d[pl.ds(b, 1), :] = jnp.sum(jnp.where(mask, o, 0.0), axis=0, keepdims=True)
+        l2d[pl.ds(b, 1), :] = jnp.sum(jnp.where(mask, lse, 0.0), axis=0, keepdims=True)
+
+    @pl.loop(0, rows // pace)
+    def _(k):
+        for i in range(pace):
+            sequence(k * pace + i)
 
     for j in range(n_kv):
         send_part[j] = o2d[:, j * c : (j + 1) * c].astype(BF16)
@@ -361,13 +371,18 @@
     branch(nrm, g2, l2, d2, 8)
     exchange("all", [(send_all, recv_two, 4, True)])
     last = total(recv_two, n).astype(BF16)
-    own_all[...] = last
-    exchange("all", [(own_all, tbuf, 5, False)])
-    squares = jnp.zeros((rows, c), F32)
-    for i in range(n):
-        v = tbuf[i].astype(F32)
-        squares = squares + v * v
-    inv = lax.rsqrt(jnp.sum(squares, axis=1, keepdims=True) / depth + epsilon)
+    wide = last.astype(F32)
+    diagonal = lax.broadcasted_iota(jnp.int32, (rows, c), 0) == lax.broadcasted_iota(
+        jnp.int32, (rows, c), 1
+    )
+    row_sum = jnp.sum(wide * wide, axis=1, keepdims=True)
+    stat[...] = jnp.sum(jnp.where(diagonal, row_sum, 0.0), axis=0, keepdims=True)
+    exchange("all", [(stat, tbuf, 5, False)])
+    squares = tbuf[0]
+    for i in range(1, n):
+        squares = squares + tbuf[i]
+    row_sum = jnp.sum(jnp.where(diagonal, squares, 0.0), axis=1, keepdims=True)
+    inv = lax.rsqrt(row_sum / depth + epsilon)
     here = pl.ds(pl.multiple_of(me * c, c), c)
     out[...] = (mid[:, here] + 0.5 * (last.astype(F32) * inv * gains[5:6, here])).astype(BF16)
 
@@ -376,7 +391,7 @@
     tokens = args[0]
     rows, c = tokens.shape
     n = n_kv * n_tp
-    if c % 128 or args[5].shape[1] != n_kv * c or args[9].shape[1] != n_tp * c:
+    if c % 128 or rows > c or args[5].shape[1] != n_kv * c or args[9].shape[1] != n_tp * c:
         return body(*args)
     depth = n * c
     width = args[8].shape[1] * HD
@@ -390,7 +405,7 @@
         vmem((rows, depth), F32),
         vmem((rows, depth), BF16),
         vmem((rows, depth), F32),
-        vmem((8, 128), F32),
+        vmem((1, c), F32),
         vmem((rows, width), F32),
         vmem((rows, width), F32),
         vmem((rows, width), F32),
@@ -401,7 +416,7 @@
         vmem((n, *chunk), BF16),
         vmem((n, *chunk), BF16),
         vmem((n, *chunk), BF16),
-        vmem((n, *chunk), BF16),
+        vmem((n, 1, c), F32),
         vmem((n_kv, 3, *chunk), BF16),
         vmem((n_kv, 3, *chunk), BF16),
         vmem(chunk, BF16),

time: 96 us -> 92.6 us (0.965)
  Pallas kernels: 93.9 us -> 91 us
    pallas_call x1, Pallas kernels: 93.9 us -> 91 us  [layer(): pl.pallas_call(functools.partial(fused_kernel, n_kv, n_tp), out_shape=jax...]
where the time goes in v2:
time: 92.6 us; the launch traced here: 92.3 us
  Pallas kernels  91 us (98%)
  local copies, waits for them, and re-layouts  1.29 us (1%)
    pallas_call x1, Pallas kernels, layer(): pl.pallas_call(functools.partial(fused_kernel, n_kv, n_tp), out_shape=jax...  91 us

profile of v2, /device:TPU:0, one launch (start us, length us, event | category | flops | bytes accessed | tf_op | source)
XLA Modules:
  0.0 92.3 jit_solution(16983785965770178100)
XLA Ops:
  0.0 91.0 %shard_map.154 = bf16[18,128]{1,0:T(8,128)(2,1)} custom-call(bf16[18,128]{1,0:T(8,128)(2,1)} %refs_0_.1, f32[6,4096]{1,0:T(8,128)} %refs_1_.1, bf16[352,4096]{1,0:T(8,128)(2,1)} %bitcast.5, bf16[352,4096]{1,0:T(8,128)(2,1)} %bitcast.6, bf16[352,4096]{1,0:T(8,128)(2,1)} %refs_4_.1, bf16[512,1024]{1,0:T(8,128)(2,1)} %refs_5_.1, bf16[512,1024]{1,0:T(8,128)(2,1)} %refs_6_.1, ...), custom_call_target="tpu_custom_call" | custom-call | tf_op jit(solution)/shard_map/pallas_call | solution.py:441
  91.1 1.3 %copy.18 = bf16[18,128]{1,0:T(8,128)(2,1)} copy(bf16[18,128]{1,0:T(8,128)(2,1)} %shard_map.154) | data formatting | bytes 9216
